TPU v7x, 32 devices: a whole 2x2x4 slice. The times are simulated.
32 devices in a mesh: fs: 8 (over z, x), tp: 4 (over y, core).
Axes of the slice: x: 2, y: 2, z: 4, core: 2. Of those that a mesh axis runs over, the one named last changes fastest.
Arguments:
- tokens: bfloat16 [4096, 2048], P(('fs', 'tp')), may hold values from -6 to 6
- gate_weight: bfloat16 [2048, 6144], P('fs', 'tp'), may hold values from -0.125 to 0.125
- value_weight: bfloat16 [2048, 6144], P('fs', 'tp'), may hold values from -0.125 to 0.125
- gate_taps: float32 [3, 6144], P(None, 'tp'), may hold values from -3.5 to 3.5
- value_taps: float32 [3, 6144], P(None, 'tp'), may hold values from -3.5 to 3.5
- down_weight: bfloat16 [6144, 2048], P('tp', 'fs'), may hold values from -0.078125 to 0.078125
- norm_gain: float32 [2048], replicated, may hold values from 0.1 to 1.9
- norm_shift: float32 [2048], replicated, may hold values from -3 to 3
Outputs:
- mixed: bfloat16 [4096, 2048], P(('fs', 'tp'))
All inputs are finite; a program needn't handle non-finite values.
Results may differ from a plain program's by a relative error of at most 0.017.
Values may be sent and summed in bfloat16 or wider, within the bound.
A program may use at most 256 MiB of HBM per device.

v0:
```python
import functools

import jax
import jax.numpy as jnp
from jax import lax
from jax.experimental import pallas as pl
from jax.experimental.pallas import tpu as pltpu
from jax.sharding import PartitionSpec as P

MESH = pl.DeviceIdType.MESH
LEAD = 8


def kernel(
    dims,
    x_ref, g_ref, v_ref, gt_ref, vt_ref, d_ref, gain_ref, shift_ref,
    out_ref,
    tok, gw, vw, dw, pre_g, pre_v, hid, part, rc, ry, zr,
    tok_r, tz_s, ty_s, tc_s, w_r, wz_s, wx_s, rc_r, rc_s, ry_r, ry_s, zc_r, zc_s,
):
    nz, nx, ny, nc = dims
    rows, width = x_ref.shape
    depth = g_ref.shape[0]
    units = gw.shape[1]
    cols = d_ref.shape[1]
    fs = lax.axis_index("fs")
    tp = lax.axis_index("tp")
    z, x = fs // nx, fs % nx
    y, c = tp // nc, tp % nc
    length = ny * nc * rows

    def at(zz=z, xx=x, yy=y, cc=c):
        return {"fs": zz * nx + xx, "tp": yy * nc + cc}

    z_others = [(z + i) % nz for i in range(1, nz)]
    x_others = [(x + i) % nx for i in range(1, nx)]
    y_others = [(y + i) % ny for i in range(1, ny)]
    c_others = [(c + i) % nc for i in range(1, nc)]

    barrier = pltpu.get_barrier_semaphore()
    partners = (
        [at(zz=i) for i in z_others]
        + [at(xx=i) for i in x_others]
        + [at(yy=i) for i in y_others]
        + [at(cc=i) for i in c_others]
    )
    for partner in partners:
        pl.semaphore_signal(barrier, inc=1, device_id=partner, device_id_type=MESH)
    pl.semaphore_wait(barrier, len(partners))

    def copy(src, dst, send, recv, device):
        return pltpu.make_async_remote_copy(
            src_ref=src, dst_ref=dst, send_sem=send, recv_sem=recv,
            device_id=device, device_id_type=MESH,
        )

    def slot(zz, t):
        return tok.at[zz, pl.ds(pl.multiple_of(t * rows, rows), rows)]

    def tok_copy(src, zz, t, send, device):
        return copy(src, slot(zz, t), send, tok_r.at[zz, t], device)

    def tok_z(src, zz, way):
        return tok_copy(src, zz, tp, tz_s.at[way, zz], at(zz=z + 1 - 2 * way))

    def tok_y(src, zz, yy):
        return tok_copy(src, zz, tp, ty_s.at[zz, yy], at(yy=yy))

    def tok_c(src, zz, yy, cc):
        return tok_copy(src, zz, yy * nc + c, tc_s.at[zz, yy, cc], at(cc=cc))

    def tok_wait(zz, t):
        tok_copy(slot(zz, t), zz, t, tz_s.at[0, 0], partners[0]).wait_recv()

    def spread(src, zz):
        for yy in y_others:
            tok_y(src, zz, yy).start()
        for cc in c_others:
            tok_c(src, zz, y, cc).start()

    def piece(kind, zz):
        if kind == 2:
            return d_ref.at[pl.ds(pl.multiple_of(zz * units, 128), units)]
        ref = g_ref if kind == 0 else v_ref
        return ref.at[:, pl.ds(pl.multiple_of(zz * units, 128), units)]

    def place(kind, src):
        if kind == 2:
            return dw.at[:, pl.ds(pl.multiple_of(src * cols, cols), cols)]
        ref = gw if kind == 0 else vw
        return ref.at[pl.ds(pl.multiple_of(src * depth, depth), depth)]

    def w_z(kind, zz):
        return copy(piece(kind, zz), place(kind, fs), wz_s.at[kind, zz], w_r.at[kind, fs], at(zz=zz))

    def w_x(kind, src, zz, xx):
        return copy(src, place(kind, zz * nx + x), wx_s.at[kind, zz, xx], w_r.at[kind, zz * nx + x], at(xx=xx))

    def w_wait(kind, src):
        copy(place(kind, src), place(kind, src), wz_s.at[kind, 0], w_r.at[kind, src], partners[0]).wait_recv()

    def w_own(kind):
        for xx in x_others:
            w_x(kind, piece(kind, z), z, xx).start()

    def both(step, act):
        for way in range(2):
            zz = z - step + 2 * step * way

            @pl.when((zz >= 0) & (zz < nz))
            def _():
                act(zz)

    def w_send(kind):
        for step in range(1, nz):
            both(step, lambda zz: w_z(kind, zz).start())

    def w_forward(kind, step):
        def act(zz):
            w_wait(kind, zz * nx + x)
            for xx in x_others:
                w_x(kind, place(kind, zz * nx + x), zz, xx).start()

        both(step, act)

    def relay(step):
        for way in range(2):
            zz = z - step + 2 * step * way

            @pl.when((zz >= 0) & (zz < nz))
            def _():
                tok_wait(zz, tp)
                if step < nz - 1:
                    ahead = z + 1 - 2 * way

                    @pl.when((ahead >= 0) & (ahead < nz))
                    def _():
                        tok_z(slot(zz, tp), zz, way).start()
                spread(slot(zz, tp), zz)

    for way in range(2):
        ahead = z + 1 - 2 * way

        @pl.when((ahead >= 0) & (ahead < nz))
        def _():
            tok_z(x_ref, z, way).start()

    w_own(0)
    spread(x_ref, z)
    w_own(1)
    tok[z, pl.ds(pl.multiple_of(tp * rows, rows), rows)] = x_ref[...]
    mine = pl.ds(pl.multiple_of(fs * depth, depth), depth)
    part_units = pl.ds(pl.multiple_of(z * units, 128), units)
    gw[mine, :] = g_ref[:, part_units]
    vw[mine, :] = v_ref[:, part_units]
    dw[:, pl.ds(pl.multiple_of(fs * cols, cols), cols)] = d_ref[part_units, :]
    for step in range(1, nz):
        relay(step)
        if step == min(2, nz - 1):
            for kind in range(3):
                w_send(kind)
            w_own(2)
    for kind in range(2):
        for step in range(1, nz):
            w_forward(kind, step)

    half = (2 * z) // nz if nz > 1 else 0
    near = z + half * (nz - 1 - 2 * z)

    def order(j):
        past = (j - near - 1 + nz) // nz
        f = past * j + (1 - past) * (near - j)
        return f + half * (nz - 1 - 2 * f)

    def far_order(k):
        return order(nz - 1 - k)

    def cross(zz):
        for yy in y_others:
            tok_wait(zz, yy * nc + c)
            for cc in c_others:
                tok_c(slot(zz, yy * nc + c), zz, yy, cc).start()

    cross(order(0))
    for kind in range(2):
        for xx in x_others:
            for i in range(nz):
                w_wait(kind, i * nx + xx)

    def block(zz, t):
        return part.at[zz, pl.ds(pl.multiple_of(t * rows, rows), rows)]

    def rc_copy(zz, yy, cc):
        return copy(block(zz, yy * nc + cc), rc.at[zz, yy], rc_s.at[zz, yy], rc_r.at[zz, yy], at(cc=cc))

    def ry_copy(zz, yy):
        return copy(block(zz, yy * nc + c), ry.at[zz, y], ry_s.at[zz, yy], ry_r.at[zz, y], at(yy=yy))

    def ry_wait(zz, yy):
        copy(block(zz, tp), ry.at[zz, yy], ry_s.at[zz, yy], ry_r.at[zz, yy], partners[0]).wait_recv()

    def zc_copy(way, zz):
        return copy(block(zz, tp), zr.at[way, zz], zc_s.at[way, zz], zc_r.at[way, zz], at(zz=z + 1 - 2 * way))

    def zc_wait(way, zz):
        copy(block(zz, tp), zr.at[way, zz], zc_s.at[way, zz], zc_r.at[way, zz], partners[0]).wait_recv()

    def mix(pre, w, taps, zz):
        raw = jnp.dot(tok[zz], w[...], preferred_element_type=jnp.float32)
        pre[pl.ds(LEAD, length), :] = raw.astype(jnp.bfloat16).astype(jnp.float32)
        return (
            taps[0:1, part_units] * pre[pl.ds(LEAD - 2, length), :]
            + taps[1:2, part_units] * pre[pl.ds(LEAD - 1, length), :]
            + taps[2:3, part_units] * pre[pl.ds(LEAD, length), :]
        )

    pre_g[0:LEAD, :] = jnp.zeros((LEAD, units), jnp.float32)
    pre_v[0:LEAD, :] = jnp.zeros((LEAD, units), jnp.float32)

    def f32(ref):
        return ref[...].astype(jnp.float32)

    for k in range(nz):
        zz = order(k)
        if k + 1 < nz:
            cross(order(k + 1))
        for yy in range(ny):
            for cc in c_others:
                tok_wait(zz, yy * nc + cc)
        gate = mix(pre_g, gw, gt_ref, zz)
        value = mix(pre_v, vw, vt_ref, zz)
        act = 0.5 * gate * (1.0 + lax.erf(gate * (0.5**0.5)))
        hid[zz] = (act * value).astype(jnp.bfloat16)
        if k + 1 < nz:
            w_forward(2, k + 1)
    for xx in x_others:
        for i in range(nz):
            w_wait(2, i * nx + xx)

    def body(k, carry):
        @pl.when(k < nz)
        def _():
            zz = far_order(k)
            part[zz] = jnp.dot(hid[zz], dw[...], preferred_element_type=jnp.float32).astype(jnp.bfloat16)
            for yy in range(ny):
                for cc in c_others:
                    rc_copy(zz, yy, cc).start()

        @pl.when((k >= 1) & (k < nz + 1))
        def _():
            zz = far_order(k - 1)
            for yy in y_others + [y]:
                if nc > 1:
                    rc_copy(zz, yy, c_others[0]).wait_recv()
                    mine = block(zz, yy * nc + c)
                    mine[...] = (f32(mine) + f32(rc.at[zz, yy])).astype(jnp.bfloat16)
            for yy in y_others:
                ry_copy(zz, yy).start()

        @pl.when(k >= 2)
        def _():
            zz = far_order(k - 2)
            mine = block(zz, tp)
            total = f32(mine)
            for yy in y_others:
                ry_wait(zz, yy)
                total = total + f32(ry.at[zz, yy])
            mine[...] = total.astype(jnp.bfloat16)
            t = k - 2
            for way in range(2):
                pos = z + way * (nz - 1 - 2 * z)
                far = nz - 1 - t + pos
                dest = far + way * (nz - 1 - 2 * far)

                @pl.when((t < nz - 1) & (t >= pos) & (pos < nz - 1))
                def _():
                    @pl.when(pos > 0)
                    def _():
                        zc_wait(way, dest)
                        sent = block(dest, tp)
                        sent[...] = (f32(sent) + f32(zr.at[way, dest])).astype(jnp.bfloat16)

                    zc_copy(way, dest).start()

        return carry

    lax.fori_loop(0, nz + 2, body, 0)

    for way in range(2):
        back = z - 1 + 2 * way

        @pl.when((back >= 0) & (back < nz))
        def _():
            zc_wait(way, z)

        @pl.when((back < 0) | (back >= nz))
        def _():
            zr[way, z] = jnp.zeros((rows, width), jnp.bfloat16)

    summed = f32(block(z, tp)) + f32(zr.at[0, z]) + f32(zr.at[1, z])
    average = jnp.mean(summed, axis=1, keepdims=True)
    centered = summed - average
    variance = jnp.mean(centered * centered, axis=1, keepdims=True)
    normed = centered * lax.rsqrt(variance + 1e-05) * gain_ref[...] + shift_ref[...]
    out_ref[...] = normed.astype(out_ref.dtype)

    for way in range(2):
        ahead = z + 1 - 2 * way

        @pl.when((ahead >= 0) & (ahead < nz))
        def _():
            for step in range(nz - 1):
                zz = z - step + 2 * step * way

                @pl.when((zz >= 0) & (zz < nz))
                def _():
                    tok_z(slot(zz, tp), zz, way).wait_send()

                dest = z + (step + 1) * (1 - 2 * way)

                @pl.when((dest >= 0) & (dest < nz))
                def _():
                    zc_copy(way, dest).wait_send()

    for zz in range(nz):
        for yy in y_others:
            tok_y(slot(zz, tp), zz, yy).wait_send()
            ry_copy(zz, yy).wait_send()
        for yy in range(ny):
            for cc in c_others:
                tok_c(slot(zz, yy * nc + c), zz, yy, cc).wait_send()
                rc_copy(zz, yy, cc).wait_send()
    for kind in range(3):
        for zz in z_others:
            w_z(kind, zz).wait_send()
        for zz in range(nz):
            for xx in x_others:
                w_x(kind, place(kind, zz * nx + x), zz, xx).wait_send()


def solution(mesh):
    n_fs, n_tp = mesh.shape["fs"], mesh.shape["tp"]
    nc = 2 if n_tp % 2 == 0 else 1
    ny = n_tp // nc

    def local(tokens, gate_weight, value_weight, gate_taps, value_taps, down_weight, gain, shift):
        rows, width = tokens.shape
        depth, held = gate_weight.shape
        nz = 4
        while nz > 1 and (n_fs % nz or held % (128 * nz)):
            nz //= 2
        nx = n_fs // nz
        units = held // nz
        length = n_tp * rows
        bf16 = jnp.bfloat16
        dma = pltpu.SemaphoreType.DMA
        return pl.pallas_call(
            functools.partial(kernel, (nz, nx, ny, nc)),
            out_shape=jax.ShapeDtypeStruct((rows, width), bf16),
            in_specs=[pl.BlockSpec(memory_space=pltpu.VMEM)] * 8,
            out_specs=pl.BlockSpec(memory_space=pltpu.VMEM),
            scratch_shapes=[
                pltpu.VMEM((nz, length, width), bf16),
                pltpu.VMEM((width, units), bf16),
                pltpu.VMEM((width, units), bf16),
                pltpu.VMEM((units, width), bf16),
                pltpu.VMEM((length + LEAD, units), jnp.float32),
                pltpu.VMEM((length + LEAD, units), jnp.float32),
                pltpu.VMEM((nz, length, units), bf16),
                pltpu.VMEM((nz, length, width), bf16),
                pltpu.VMEM((nz, ny, rows, width), bf16),
                pltpu.VMEM((nz, ny, rows, width), bf16),
                pltpu.VMEM((2, nz, rows, width), bf16),
                dma((nz, n_tp)),
                dma((2, nz)),
                dma((nz, ny)),
                dma((nz, ny, nc)),
                dma((3, n_fs)),
                dma((3, nz)),
                dma((3, nz, nx)),
                dma((nz, ny)),
                dma((nz, ny)),
                dma((nz, ny)),
                dma((nz, ny)),
                dma((2, nz)),
                dma((2, nz)),
            ],
            compiler_params=pltpu.CompilerParams(
                collective_id=0, has_side_effects=True, vmem_limit_bytes=60 * 2**20
            ),
        )(
            tokens, gate_weight, value_weight, gate_taps, value_taps, down_weight,
            gain.reshape(1, width), shift.reshape(1, width),
        )

    in_specs = (
        P(("fs", "tp"), None),
        P("fs", "tp"),
        P("fs", "tp"),
        P(None, "tp"),
        P(None, "tp"),
        P("tp", "fs"),
        P(),
        P(),
    )
    out_specs = P(("fs", "tp"), None)
    return jax.shard_map(local, mesh=mesh, in_specs=in_specs, out_specs=out_specs, check_vma=False)
```

profile of v0, /device:TPU:0, one launch (start us, length us, event | category | flops | bytes accessed | tf_op | source)
XLA Modules:
  0.0 162.0 jit_solution(9667789392697180486)
XLA Ops:
  0.0 160.1 %shard_map.82 = bf16[128,2048]{1,0:T(8,128)(2,1)} custom-call(bf16[128,2048]{1,0:T(8,128)(2,1)} %x_ref.1, bf16[256,1536]{1,0:T(8,128)(2,1)} %g_ref.1, bf16[256,1536]{1,0:T(8,128)(2,1)} %v_ref.1, f32[3,1536]{1,0:T(4,128)} %gt_ref.1, f32[3,1536]{1,0:T(4,128)} %vt_ref.1, bf16[1536,256]{1,0:T(8,128)(2,1)} %d_ref.1, f32[1,2048]{1,0:T(1,128)} %bitcast.2, ...), custom_call_target="tpu_custom_call" | custom-call | tf_op jit(solution)/shard_map/pallas_call | solution.py:357
  160.1 1.9 %copy.10 = bf16[128,2048]{1,0:T(8,128)(2,1)} copy(bf16[128,2048]{1,0:T(8,128)(2,1)} %shard_map.82) | data formatting | bytes 1048576
where the time goes:
time: 162 us
  Pallas kernels  160 us (99%)
  local copies, waits for them, and re-layouts  1.88 us (1%)
    pallas_call x1, Pallas kernels, local(): pl.pallas_call(functools.partial(kernel, (nz, nx, ny, nc)), out_shape=jax...  160 us

commit v1 on v0

v1 whole, which is shorter than its diff:
```python
import functools

import jax
import jax.numpy as jnp
from jax import lax
from jax.experimental import pallas as pl
from jax.experimental.pallas import tpu as pltpu
from jax.sharding import PartitionSpec as P

MESH = pl.DeviceIdType.MESH
HALO = 16
BITS = 4
GV = (0, 1)
DN = (2, 3)


def kernel(
    dims,
    x_ref, g_ref, v_ref, gt_ref, vt_ref, d_ref, gain_ref, shift_ref,
    out_ref,
    tok, gw, vw, dw, taps, pre_g, pre_v, hid, part, rc, zr,
    tok_r, tz_s, tc_s, halo_r, halo_s, hc_s, tap_r, tap_s,
    w_r, wz_s, wx_s, wy_s, wf_s, rc_r, rc_s, zc_r, zc_s,
):
    nz, nx, ny, nc = dims
    rows, width = x_ref.shape
    depth = g_ref.shape[0]
    units = gw.shape[1] // ny
    cols = d_ref.shape[1]
    length = nc * rows
    bit = rows // BITS
    top = units // 2
    wide = width // 2
    fs = lax.axis_index("fs")
    tp = lax.axis_index("tp")
    z, x = fs // nx, fs % nx
    y, c = tp // nc, tp % nc

    def at(zz=z, xx=x, yy=y, cc=c):
        return {"fs": zz * nx + xx, "tp": yy * nc + cc}

    z_others = [(z + i) % nz for i in range(1, nz)]
    x_others = [(x + i) % nx for i in range(1, nx)]
    y_others = [(y + i) % ny for i in range(1, ny)]
    c_others = [(c + i) % nc for i in range(1, nc)]

    barrier = pltpu.get_barrier_semaphore()
    partners = (
        [at(zz=i) for i in z_others]
        + [at(xx=i) for i in x_others]
        + [at(yy=i) for i in y_others]
        + [at(cc=i) for i in c_others]
    )
    for partner in partners:
        pl.semaphore_signal(barrier, inc=1, device_id=partner, device_id_type=MESH)
    pl.semaphore_wait(barrier, len(partners))

    def copy(src, dst, send, recv, device):
        return pltpu.make_async_remote_copy(
            src_ref=src, dst_ref=dst, send_sem=send, recv_sem=recv,
            device_id=device, device_id_type=MESH,
        )

    def ds(start, size, unit):
        return pl.ds(pl.multiple_of(start, unit), size)

    half = (2 * z) // nz
    near = z + half * (nz - 1 - 2 * z)

    def order(j):
        past = (j - near - 1 + nz) // nz
        f = past * j + (1 - past) * (near - j)
        return f + half * (nz - 1 - 2 * f)

    def inside(zz):
        return (zz >= 0) & (zz < nz)

    def both(step, act):
        for way in range(2):
            zz = z - step + 2 * step * way

            @pl.when(inside(zz))
            def _():
                act(zz, way)

    def piece(kind, zz):
        if kind >= 2:
            return d_ref.at[ds(zz * units + (kind - 2) * top, top, 16)]
        ref = g_ref if kind == 0 else v_ref
        return ref.at[:, ds(zz * units, units, 128)]

    def place(kind, src, yy):
        if kind >= 2:
            return dw.at[ds(yy * units + (kind - 2) * top, top, 16), ds(src * cols, cols, cols)]
        ref = gw if kind == 0 else vw
        return ref.at[ds(src * depth, depth, depth), ds(yy * units, units, 128)]

    def w_z(kind, zz):
        return copy(piece(kind, zz), place(kind, fs, y), wz_s.at[kind, zz], w_r.at[kind, fs, y], at(zz=zz))

    def w_x(kind, src, zz, xx):
        s = zz * nx + x
        return copy(src, place(kind, s, y), wx_s.at[kind, zz, xx], w_r.at[kind, s, y], at(xx=xx))

    def w_y(kind, src, zz, yy):
        s = zz * nx + x
        return copy(src, place(kind, s, y), wy_s.at[kind, zz, yy], w_r.at[kind, s, y], at(yy=yy))

    def w_f(kind, zz, xx, yy):
        if kind % 2 == 0:
            s = zz * nx + xx
            return copy(place(kind, s, y), place(kind, s, y), wf_s.at[kind, zz, xx, yy], w_r.at[kind, s, y], at(yy=yy))
        s = zz * nx + x
        return copy(place(kind, s, yy), place(kind, s, yy), wf_s.at[kind, zz, xx, yy], w_r.at[kind, s, yy], at(xx=xx))

    def w_wait(kind, zz, xx, yy):
        s = zz * nx + xx
        copy(place(kind, s, yy), place(kind, s, yy), wz_s.at[kind, 0], w_r.at[kind, s, yy], partners[0]).wait_recv()

    def spread(kind, src, zz):
        for xx in x_others:
            w_x(kind, src, zz, xx).start()
        for yy in y_others:
            w_y(kind, src, zz, yy).start()

    def own(kinds):
        for kind in kinds:
            spread(kind, piece(kind, z), z)

    def arrive(kinds, zz):
        for kind in kinds:
            w_wait(kind, zz, x, y)
            spread(kind, place(kind, zz * nx + x, y), zz)

    def turn(kinds, zz):
        for kind in kinds:
            if kind % 2 == 0:
                for xx in x_others:
                    w_wait(kind, zz, xx, y)
                    for yy in y_others:
                        w_f(kind, zz, xx, yy).start()
            else:
                for yy in y_others:
                    w_wait(kind, zz, x, yy)
                    for xx in x_others:
                        w_f(kind, zz, xx, yy).start()

    def rest(kinds, zz):
        for kind in kinds:
            if kind % 2 == 0:
                for yy in y_others:
                    w_wait(kind, zz, x, yy)
            else:
                for xx in x_others:
                    w_wait(kind, zz, xx, y)
            for xx in x_others:
                for yy in y_others:
                    w_wait(kind, zz, xx, yy)

    def slot(zz, cc):
        return tok.at[zz, ds(HALO + cc * rows, rows, 16)]

    def chunk(zz, cc, b):
        return tok.at[zz, ds(HALO + cc * rows + b * bit, bit, 16)]

    def tok_z(src, zz, way, b):
        return copy(src, chunk(zz, c, b), tz_s.at[way, zz, b], tok_r.at[zz, c, b], at(zz=z + 1 - 2 * way))

    def tok_c(src, zz, cc):
        return copy(src, slot(zz, c), tc_s.at[zz, cc], tok_r.at[zz, c, 0], at(cc=cc))

    def halo_y(src, zz):
        return copy(src, tok.at[zz, pl.ds(0, HALO)], halo_s.at[zz], halo_r.at[zz], at(yy=y + 1))

    def halo_c(zz, cc):
        lead = tok.at[zz, pl.ds(0, HALO)]
        return copy(lead, lead, hc_s.at[zz, cc], halo_r.at[zz], at(cc=cc))

    def cross(src, tail, zz):
        for cc in c_others:
            tok_c(src, zz, cc).start()

        @pl.when((c == nc - 1) & (y < ny - 1))
        def _():
            halo_y(tail, zz).start()

    def tail(zz):
        return tok.at[zz, ds(HALO + (c + 1) * rows - HALO, HALO, 16)]

    def relay(step, bits):
        def act(zz, way):
            ahead = z + 1 - 2 * way
            for b in bits:
                copy(chunk(zz, c, b), chunk(zz, c, b), tz_s.at[0, 0, 0], tok_r.at[zz, c, b], partners[0]).wait_recv()
                if step < nz - 1:

                    @pl.when(inside(ahead))
                    def _():
                        tok_z(chunk(zz, c, b), zz, way, b).start()

            if bits[-1] == BITS - 1:
                cross(slot(zz, c), tail(zz), zz)

        if step < nz:
            both(step, act)

    def gathered(zz):
        for cc in c_others:
            copy(slot(zz, cc), slot(zz, cc), tz_s.at[0, 0, 0], tok_r.at[zz, cc, 0], partners[0]).wait_recv()

        @pl.when(y > 0)
        def _():
            lead = tok.at[zz, pl.ds(0, HALO)]
            copy(lead, lead, halo_s.at[zz], halo_r.at[zz], partners[0]).wait_recv()

            @pl.when(c == nc - 1)
            def _():
                for cc in c_others:
                    halo_c(zz, cc).start()

    def tap(kind, yy):
        ref = gt_ref if kind == 0 else vt_ref
        return copy(
            ref.at[:, ds(z * units, units, 128)], taps.at[kind, :, ds(y * units, units, 128)],
            tap_s.at[kind, yy], tap_r.at[kind, y], at(yy=yy),
        )

    def tap_wait(kind, yy):
        dst = taps.at[kind, :, ds(yy * units, units, 128)]
        copy(dst, dst, tap_s.at[kind, yy], tap_r.at[kind, yy], partners[0]).wait_recv()

    for step in range(1, nz):
        both(step, lambda zz, way: [w_z(kind, zz).start() for kind in GV])
    own(GV)
    for kind in range(2):
        for yy in y_others:
            tap(kind, yy).start()
    cross(x_ref, x_ref.at[pl.ds(rows - HALO, HALO)], z)

    def middle(way):
        return z + way * (nz - 1 - 2 * z) == nz // 2 - 1

    def down_near(late):
        for way in range(2):
            dest = z + 1 - 2 * way
            wanted = middle(way) if late else jnp.logical_not(middle(way))

            @pl.when(inside(dest) & wanted)
            def _():
                for kind in DN:
                    w_z(kind, dest).start()

    for way in range(2):

        @pl.when(inside(z + 1 - 2 * way))
        def _():
            for b in range(BITS):
                tok_z(x_ref.at[pl.ds(b * bit, bit)], z, way, b).start()

    down_near(False)

    @pl.when(y == 0)
    def _():
        tok[:, 0:HALO, :] = jnp.zeros((nz, HALO, width), jnp.bfloat16)

    tok[z, ds(HALO + c * rows, rows, 16)] = x_ref[...]
    mine = ds(fs * depth, depth, depth)
    here = ds(y * units, units, 128)
    part_units = ds(z * units, units, 128)
    gw[mine, here] = g_ref[:, part_units]
    vw[mine, here] = v_ref[:, part_units]
    dw[here, ds(fs * cols, cols, cols)] = d_ref[part_units, :]
    taps[0, :, here] = gt_ref[:, part_units]
    taps[1, :, here] = vt_ref[:, part_units]

    for k in range(1, nz):
        arrive(GV, order(k))
        turn(GV, order(k - 1))
    relay(1, range(BITS))
    down_near(True)
    turn(GV, order(nz - 1))
    own(DN)
    side = nz // 2
    for k in range(1, side):
        arrive(DN, order(k))
    relay(2, range(BITS // 2))
    for kind in range(2):
        for yy in y_others:
            tap_wait(kind, yy)
    for k in range(nz):
        rest(GV, order(k))

    def f32(ref):
        return ref[...].astype(jnp.float32)

    def mix(pre, w, kind, zz):
        raw = jnp.dot(tok[zz], w[...], preferred_element_type=jnp.float32)
        pre[...] = raw.astype(jnp.bfloat16).astype(jnp.float32)
        return (
            taps[kind, 0:1, :] * pre[pl.ds(HALO - 2, length), :]
            + taps[kind, 1:2, :] * pre[pl.ds(HALO - 1, length), :]
            + taps[kind, 2:3, :] * pre[pl.ds(HALO, length), :]
        )

    def hidden(zz):
        gathered(zz)
        gate = mix(pre_g, gw, 0, zz)
        value = mix(pre_v, vw, 1, zz)
        act = 0.5 * gate * (1.0 + lax.erf(gate * (0.5**0.5)))
        hid[zz] = (act * value).astype(jnp.bfloat16)

    def wing(h):
        return ds(h * wide, wide, wide)

    def block(zz, cc, h):
        return part.at[zz, ds(cc * rows, rows, rows), wing(h)]

    def rc_copy(zz, cc, h):
        return copy(block(zz, cc, h), rc.at[zz, :, wing(h)], rc_s.at[zz, cc, h], rc_r.at[zz, h], at(cc=cc))

    def zc_copy(way, zz, h):
        return copy(block(zz, c, h), zr.at[way, zz, :, wing(h)], zc_s.at[way, zz, h], zc_r.at[way, zz, h], at(zz=z + 1 - 2 * way))

    def zc_wait(way, zz, h):
        dst = zr.at[way, zz, :, wing(h)]
        copy(dst, dst, zc_s.at[way, zz, h], zc_r.at[way, zz, h], partners[0]).wait_recv()

    def product(zz, h):
        part[zz, :, wing(h)] = jnp.dot(
            hid[zz], dw[:, wing(h)], preferred_element_type=jnp.float32
        ).astype(jnp.bfloat16)
        for cc in c_others:
            rc_copy(zz, cc, h).start()

    def pair(zz, h, first):
        for _ in c_others:
            rc_copy(zz, c, h).wait_recv()
            sent = block(zz, c, h)
            sent[...] = (f32(sent) + f32(rc.at[zz, :, wing(h)])).astype(jnp.bfloat16)
        if first:

            @pl.when((z == 0) | (z == nz - 1))
            def _():
                zc_copy(half, zz, h).start()

    def pass_on(pos, j, e):
        way = jnp.where(z == pos, 0, 1)
        dest = z + j * (1 - 2 * way)
        h = e + way * (1 - 2 * e)

        @pl.when((z == pos) | (z == nz - 1 - pos))
        def _():
            zc_wait(way, dest, h)
            sent = block(dest, c, h)
            sent[...] = (f32(sent) + f32(zr.at[way, dest, :, wing(h)])).astype(jnp.bfloat16)
            zc_copy(way, dest, h).start()

    def down_far():
        for step in range(2, nz):
            both(step, lambda zz, way: [w_z(kind, zz).start() for kind in DN])

    def down_ready(ks):
        for k in ks:
            rest(DN, order(k))

    hidden(order(0))
    down_far()
    turn(DN, order(0))
    relay(2, range(BITS // 2, BITS))
    hidden(order(1))
    for k in range(1, side):
        turn(DN, order(k))
    down_ready(range(side))
    product(order(1), half)
    for k in range(2, nz):
        if k > 2:
            relay(k, range(BITS))
        hidden(order(k))
        pair(order(k - 1), half, True)
        product(order(k), half)
    product(order(0), half)
    pair(order(nz - 1), half, True)
    pair(order(0), half, False)

    for k in range(side, nz):
        arrive(DN, order(k))
        turn(DN, order(k))
    for pos in range(1, nz // 2):
        pass_on(pos, 1, 0)
    down_ready(range(side, nz))
    other = 1 - half
    for k in range(nz):
        product(order(nz - 1 - k), other)
        if k > 0:
            pair(order(nz - k), other, True)
    pair(order(0), other, False)
    for pos in range(1, nz // 2):
        for j in range(2, nz - pos):
            pass_on(pos, j, 0)
        for j in range(nz - pos - 1, 1, -1):
            pass_on(pos, j, 1)
    for pos in range(nz // 2, nz - 1):
        for j in range(1, nz - pos):
            pass_on(pos, j, 0)
    for pos in range(1, nz // 2):
        pass_on(pos, 1, 1)
    for pos in range(nz // 2, nz - 1):
        for j in range(nz - pos - 1, 0, -1):
            pass_on(pos, j, 1)

    for way in range(2):
        back = z - 1 + 2 * way

        @pl.when(inside(back))
        def _():
            for h in range(2):
                zc_wait(way, z, h)

        @pl.when(jnp.logical_not(inside(back)))
        def _():
            zr[way, z] = jnp.zeros((rows, width), jnp.bfloat16)

    summed = f32(part.at[z, ds(c * rows, rows, rows)]) + f32(zr.at[0, z]) + f32(zr.at[1, z])
    average = jnp.mean(summed, axis=1, keepdims=True)
    centered = summed - average
    variance = jnp.mean(centered * centered, axis=1, keepdims=True)
    normed = centered * lax.rsqrt(variance + 1e-05) * gain_ref[...] + shift_ref[...]
    out_ref[...] = normed.astype(out_ref.dtype)

    for way in range(2):

        @pl.when(inside(z + 1 - 2 * way))
        def _():
            for step in range(nz - 1):
                zz = z - step + 2 * step * way

                @pl.when(inside(zz))
                def _():
                    for b in range(BITS):
                        tok_z(chunk(zz, c, b), zz, way, b).wait_send()

                dest = z + (step + 1) * (1 - 2 * way)

                @pl.when(inside(dest))
                def _():
                    for h in range(2):
                        zc_copy(way, dest, h).wait_send()

    for zz in range(nz):
        for cc in c_others:
            tok_c(slot(zz, c), zz, cc).wait_send()
            for h in range(2):
                rc_copy(zz, cc, h).wait_send()

        @pl.when((c == nc - 1) & (y < ny - 1))
        def _():
            halo_y(tail(zz), zz).wait_send()

        @pl.when((c == nc - 1) & (y > 0))
        def _():
            for cc in c_others:
                halo_c(zz, cc).wait_send()

    for kind in range(2):
        for yy in y_others:
            tap(kind, yy).wait_send()
    for kind in GV + DN:
        for zz in z_others:
            w_z(kind, zz).wait_send()
        for zz in range(nz):
            src = place(kind, zz * nx + x, y)
            for xx in x_others:
                w_x(kind, src, zz, xx).wait_send()
            for yy in y_others:
                w_y(kind, src, zz, yy).wait_send()
            for xx in x_others:
                for yy in y_others:
                    w_f(kind, zz, xx, yy).wait_send()


def solution(mesh):
    n_fs, n_tp = mesh.shape["fs"], mesh.shape["tp"]
    nc = 2 if n_tp % 2 == 0 else 1
    ny = n_tp // nc

    def local(tokens, gate_weight, value_weight, gate_taps, value_taps, down_weight, gain, shift):
        rows, width = tokens.shape
        depth, held = gate_weight.shape
        count = gate_taps.shape[0]
        nz = 4
        while nz > 2 and (n_fs % nz or held % (128 * nz)):
            nz //= 2
        nx = n_fs // nz
        units = held // nz
        length = nc * rows
        bf16 = jnp.bfloat16
        dma = pltpu.SemaphoreType.DMA
        return pl.pallas_call(
            functools.partial(kernel, (nz, nx, ny, nc)),
            out_shape=jax.ShapeDtypeStruct((rows, width), bf16),
            in_specs=[pl.BlockSpec(memory_space=pltpu.VMEM)] * 8,
            out_specs=pl.BlockSpec(memory_space=pltpu.VMEM),
            scratch_shapes=[
                pltpu.VMEM((nz, HALO + length, width), bf16),
                pltpu.VMEM((width, ny * units), bf16),
                pltpu.VMEM((width, ny * units), bf16),
                pltpu.VMEM((ny * units, width), bf16),
                pltpu.VMEM((2, count, ny * units), jnp.float32),
                pltpu.VMEM((HALO + length, ny * units), jnp.float32),
                pltpu.VMEM((HALO + length, ny * units), jnp.float32),
                pltpu.VMEM((nz, length, ny * units), bf16),
                pltpu.VMEM((nz, length, width), bf16),
                pltpu.VMEM((nz, rows, width), bf16),
                pltpu.VMEM((2, nz, rows, width), bf16),
                dma((nz, nc, BITS)),
                dma((2, nz, BITS)),
                dma((nz, nc)),
                dma((nz,)),
                dma((nz,)),
                dma((nz, nc)),
                dma((2, ny)),
                dma((2, ny)),
                dma((4, n_fs, ny)),
                dma((4, nz)),
                dma((4, nz, nx)),
                dma((4, nz, ny)),
                dma((4, nz, nx, ny)),
                dma((nz, 2)),
                dma((nz, nc, 2)),
                dma((2, nz, 2)),
                dma((2, nz, 2)),
            ],
            compiler_params=pltpu.CompilerParams(
                collective_id=0, has_side_effects=True, vmem_limit_bytes=60 * 2**20
            ),
        )(
            tokens, gate_weight, value_weight, gate_taps, value_taps, down_weight,
            gain.reshape(1, width), shift.reshape(1, width),
        )

    in_specs = (
        P(("fs", "tp"), None),
        P("fs", "tp"),
        P("fs", "tp"),
        P(None, "tp"),
        P(None, "tp"),
        P("tp", "fs"),
        P(),
        P(),
    )
    out_specs = P(("fs", "tp"), None)
    return jax.shard_map(local, mesh=mesh, in_specs=in_specs, out_specs=out_specs, check_vma=False)
```

time: 162 us -> 142 us (0.88)
  Pallas kernels: 160 us -> 140 us
    pallas_call x1, Pallas kernels: 160 us -> 140 us  [local(): pl.pallas_call(functools.partial(kernel, (nz, nx, ny, nc)), out_shape=jax...]
where the time goes in v1:
time: 142 us
  Pallas kernels  140 us (99%)
  local copies, waits for them, and re-layouts  1.88 us (1%)
    pallas_call x1, Pallas kernels, local(): pl.pallas_call(functools.partial(kernel, (nz, nx, ny, nc)), out_shape=jax...  140 us

profile of v1, /device:TPU:0, one launch (start us, length us, event | category | flops | bytes accessed | tf_op | source)
XLA Modules:
  0.0 142.0 jit_solution(10831699534004015622)
XLA Ops:
  0.0 140.1 %shard_map.82 = bf16[128,2048]{1,0:T(8,128)(2,1)} custom-call(bf16[128,2048]{1,0:T(8,128)(2,1)} %x_ref.1, bf16[256,1536]{1,0:T(8,128)(2,1)} %g_ref.1, bf16[256,1536]{1,0:T(8,128)(2,1)} %v_ref.1, f32[3,1536]{1,0:T(4,128)} %gt_ref.1, f32[3,1536]{1,0:T(4,128)} %vt_ref.1, bf16[1536,256]{1,0:T(8,128)(2,1)} %d_ref.1, f32[1,2048]{1,0:T(1,128)} %bitcast.2, ...), custom_call_target="tpu_custom_call" | custom-call | tf_op jit(solution)/shard_map/pallas_call | solution.py:498
  140.1 1.9 %copy.10 = bf16[128,2048]{1,0:T(8,128)(2,1)} copy(bf16[128,2048]{1,0:T(8,128)(2,1)} %shard_map.82) | data formatting | bytes 1048576

commit v2 on v1

--- a/solution.py
+++ b/solution.py
@@ -19,7 +19,7 @@
     x_ref, g_ref, v_ref, gt_ref, vt_ref, d_ref, gain_ref, shift_ref,
     out_ref,
     tok, gw, vw, dw, taps, pre_g, pre_v, hid, part, rc, zr,
-    tok_r, tz_s, tc_s, halo_r, halo_s, hc_s, tap_r, tap_s,
+    tok_r, tz_s, tc_s, halo_r, halo_s, hz_s, hc_s, tap_r, tap_s,
     w_r, wz_s, wx_s, wy_s, wf_s, rc_r, rc_s, zc_r, zc_s,
 ):
     nz, nx, ny, nc = dims
@@ -30,7 +30,7 @@
     length = nc * rows
     bit = rows // BITS
     top = units // 2
-    wide = width // 2
+    wide = nx * cols
     fs = lax.axis_index("fs")
     tp = lax.axis_index("tp")
     z, x = fs // nx, fs % nx
@@ -72,8 +72,26 @@
         f = past * j + (1 - past) * (near - j)
         return f + half * (nz - 1 - 2 * f)
 
+    ends = (z == 0) | (z == nz - 1)
+
+    def early(k):
+        return jnp.where(ends, order(3 - k), order(k)) if nz > 2 and k in (1, 2) else order(k)
+
+    def late(k):
+        return order(5 - k) if nz > 2 and k in (2, 3) else order(k)
+
     def inside(zz):
         return (zz >= 0) & (zz < nz)
+
+    def inner(act):
+        @pl.when(jnp.logical_not(ends))
+        def _():
+            act()
+
+    def outer(act):
+        @pl.when(ends)
+        def _():
+            act()
 
     def both(step, act):
         for way in range(2):
@@ -169,54 +187,67 @@
     def tok_c(src, zz, cc):
         return copy(src, slot(zz, c), tc_s.at[zz, cc], tok_r.at[zz, c, 0], at(cc=cc))
 
-    def halo_y(src, zz):
-        return copy(src, tok.at[zz, pl.ds(0, HALO)], halo_s.at[zz], halo_r.at[zz], at(yy=y + 1))
+    keeper = (c == nc - 1) & (y > 0)
+
+    def lead(zz):
+        return tok.at[zz, pl.ds(0, HALO)]
+
+    def halo_y():
+        return copy(x_ref.at[pl.ds(rows - HALO, HALO)], lead(z), halo_s.at[z], halo_r.at[z], at(yy=y + 1))
+
+    def halo_z(zz, way):
+        return copy(lead(zz), lead(zz), hz_s.at[way, zz], halo_r.at[zz], at(zz=z + 1 - 2 * way))
 
     def halo_c(zz, cc):
-        lead = tok.at[zz, pl.ds(0, HALO)]
-        return copy(lead, lead, hc_s.at[zz, cc], halo_r.at[zz], at(cc=cc))
-
-    def cross(src, tail, zz):
+        return copy(lead(zz), lead(zz), hc_s.at[zz, cc], halo_r.at[zz], at(cc=cc))
+
+    def halo_wait(zz):
+        copy(lead(zz), lead(zz), hc_s.at[zz, 0], halo_r.at[zz], partners[0]).wait_recv()
+
+    def keep(zz, ways, further):
+        @pl.when(keeper)
+        def _():
+            halo_wait(zz)
+            if further:
+                for way in ways:
+
+                    @pl.when(inside(z + 1 - 2 * way))
+                    def _():
+                        halo_z(zz, way).start()
+
+            for cc in c_others:
+                halo_c(zz, cc).start()
+
+    def cross(src, zz):
         for cc in c_others:
             tok_c(src, zz, cc).start()
 
-        @pl.when((c == nc - 1) & (y < ny - 1))
-        def _():
-            halo_y(tail, zz).start()
-
-    def tail(zz):
-        return tok.at[zz, ds(HALO + (c + 1) * rows - HALO, HALO, 16)]
-
     def relay(step, bits):
-        def act(zz, way):
+        for way in (half, 1 - half):
+            zz = z - step + 2 * step * way
             ahead = z + 1 - 2 * way
-            for b in bits:
-                copy(chunk(zz, c, b), chunk(zz, c, b), tz_s.at[0, 0, 0], tok_r.at[zz, c, b], partners[0]).wait_recv()
-                if step < nz - 1:
-
-                    @pl.when(inside(ahead))
-                    def _():
-                        tok_z(chunk(zz, c, b), zz, way, b).start()
-
-            if bits[-1] == BITS - 1:
-                cross(slot(zz, c), tail(zz), zz)
-
-        if step < nz:
-            both(step, act)
+
+            @pl.when(inside(zz))
+            def _():
+                for b in bits:
+                    copy(chunk(zz, c, b), chunk(zz, c, b), tz_s.at[0, 0, 0], tok_r.at[zz, c, b], partners[0]).wait_recv()
+                    if step < nz - 1:
+
+                        @pl.when(inside(ahead))
+                        def _():
+                            tok_z(chunk(zz, c, b), zz, way, b).start()
+
+                if bits[-1] == BITS - 1:
+                    cross(slot(zz, c), zz)
+                    keep(zz, (way,), step < nz - 1)
 
     def gathered(zz):
         for cc in c_others:
             copy(slot(zz, cc), slot(zz, cc), tz_s.at[0, 0, 0], tok_r.at[zz, cc, 0], partners[0]).wait_recv()
 
-        @pl.when(y > 0)
-        def _():
-            lead = tok.at[zz, pl.ds(0, HALO)]
-            copy(lead, lead, halo_s.at[zz], halo_r.at[zz], partners[0]).wait_recv()
-
-            @pl.when(c == nc - 1)
-            def _():
-                for cc in c_others:
-                    halo_c(zz, cc).start()
+        @pl.when((y > 0) & (c < nc - 1))
+        def _():
+            halo_wait(zz)
 
     def tap(kind, yy):
         ref = gt_ref if kind == 0 else vt_ref
@@ -229,35 +260,41 @@
         dst = taps.at[kind, :, ds(yy * units, units, 128)]
         copy(dst, dst, tap_s.at[kind, yy], tap_r.at[kind, yy], partners[0]).wait_recv()
 
-    for step in range(1, nz):
-        both(step, lambda zz, way: [w_z(kind, zz).start() for kind in GV])
+    def place_of(way):
+        return z + way * (nz - 1 - 2 * z)
+
+    def line(kinds, way, steps, wanted=True):
+        for step in steps:
+            zz = z + step * (1 - 2 * way)
+
+            @pl.when(inside(zz) & wanted)
+            def _():
+                for kind in kinds:
+                    w_z(kind, zz).start()
+
+    central = nz // 2 - 1
+
+    @pl.when((c == nc - 1) & (y < ny - 1))
+    def _():
+        halo_y().start()
+
     own(GV)
+    for way in range(2):
+        pos = place_of(way)
+        line(GV, way, (1,), pos == 0)
+        line(GV, way, range(nz - 1, 0, -1), pos > 0)
+
+        @pl.when(inside(z + 1 - 2 * way))
+        def _():
+            for b in range(BITS):
+                tok_z(x_ref.at[pl.ds(b * bit, bit)], z, way, b).start()
+
+        line(GV, way, range(nz - 1, 1, -1), pos == 0)
+        line(DN, way, (1,), pos != central)
     for kind in range(2):
         for yy in y_others:
             tap(kind, yy).start()
-    cross(x_ref, x_ref.at[pl.ds(rows - HALO, HALO)], z)
-
-    def middle(way):
-        return z + way * (nz - 1 - 2 * z) == nz // 2 - 1
-
-    def down_near(late):
-        for way in range(2):
-            dest = z + 1 - 2 * way
-            wanted = middle(way) if late else jnp.logical_not(middle(way))
-
-            @pl.when(inside(dest) & wanted)
-            def _():
-                for kind in DN:
-                    w_z(kind, dest).start()
-
-    for way in range(2):
-
-        @pl.when(inside(z + 1 - 2 * way))
-        def _():
-            for b in range(BITS):
-                tok_z(x_ref.at[pl.ds(b * bit, bit)], z, way, b).start()
-
-    down_near(False)
+    cross(x_ref, z)
 
     @pl.when(y == 0)
     def _():
@@ -273,17 +310,24 @@
     taps[0, :, here] = gt_ref[:, part_units]
     taps[1, :, here] = vt_ref[:, part_units]
 
+    keep(z, range(2), True)
+    side = nz // 2
     for k in range(1, nz):
-        arrive(GV, order(k))
-        turn(GV, order(k - 1))
+        if k == nz - 1:
+            turn(GV, early(k - 1))
+        arrive(GV, early(k))
+        if k < nz - 1:
+            turn(GV, early(k - 1))
     relay(1, range(BITS))
-    down_near(True)
+    for way in range(2):
+        line(DN, way, range(nz - 1, 0, -1), place_of(way) == central)
     turn(GV, order(nz - 1))
     own(DN)
-    side = nz // 2
-    for k in range(1, side):
-        arrive(DN, order(k))
-    relay(2, range(BITS // 2))
+    for way in range(2):
+        line(DN, way, range(2, nz), place_of(way) < central)
+    if nz > 2:
+        arrive(DN[:1], order(1))
+        outer(lambda: relay(2, range(BITS)))
     for kind in range(2):
         for yy in y_others:
             tap_wait(kind, yy)
@@ -332,21 +376,22 @@
         for cc in c_others:
             rc_copy(zz, cc, h).start()
 
-    def pair(zz, h, first):
+    def pair(zz, h):
         for _ in c_others:
             rc_copy(zz, c, h).wait_recv()
             sent = block(zz, c, h)
             sent[...] = (f32(sent) + f32(rc.at[zz, :, wing(h)])).astype(jnp.bfloat16)
-        if first:
-
-            @pl.when((z == 0) | (z == nz - 1))
-            def _():
-                zc_copy(half, zz, h).start()
+
+    def leave(zz, h):
+        @pl.when(ends)
+        def _():
+            zc_copy(half, zz, h).start()
 
     def pass_on(pos, j, e):
         way = jnp.where(z == pos, 0, 1)
         dest = z + j * (1 - 2 * way)
-        h = e + way * (1 - 2 * e)
+        e = 5 - e if e > 1 else e
+        h = e + way * (nz - 1 - 2 * e)
 
         @pl.when((z == pos) | (z == nz - 1 - pos))
         def _():
@@ -355,77 +400,95 @@
             sent[...] = (f32(sent) + f32(zr.at[way, dest, :, wing(h)])).astype(jnp.bfloat16)
             zc_copy(way, dest, h).start()
 
-    def down_far():
-        for step in range(2, nz):
-            both(step, lambda zz, way: [w_z(kind, zz).start() for kind in DN])
-
-    def down_ready(ks):
-        for k in ks:
-            rest(DN, order(k))
-
-    hidden(order(0))
-    down_far()
-    turn(DN, order(0))
-    relay(2, range(BITS // 2, BITS))
-    hidden(order(1))
-    for k in range(1, side):
-        turn(DN, order(k))
-    down_ready(range(side))
-    product(order(1), half)
-    for k in range(2, nz):
-        if k > 2:
-            relay(k, range(BITS))
-        hidden(order(k))
-        pair(order(k - 1), half, True)
-        product(order(k), half)
-    product(order(0), half)
-    pair(order(nz - 1), half, True)
-    pair(order(0), half, False)
-
-    for k in range(side, nz):
-        arrive(DN, order(k))
-        turn(DN, order(k))
-    for pos in range(1, nz // 2):
-        pass_on(pos, 1, 0)
-    down_ready(range(side, nz))
-    other = 1 - half
-    for k in range(nz):
-        product(order(nz - 1 - k), other)
-        if k > 0:
-            pair(order(nz - k), other, True)
-    pair(order(0), other, False)
-    for pos in range(1, nz // 2):
-        for j in range(2, nz - pos):
-            pass_on(pos, j, 0)
-        for j in range(nz - pos - 1, 1, -1):
-            pass_on(pos, j, 1)
-    for pos in range(nz // 2, nz - 1):
-        for j in range(1, nz - pos):
-            pass_on(pos, j, 0)
-    for pos in range(1, nz // 2):
-        pass_on(pos, 1, 1)
-    for pos in range(nz // 2, nz - 1):
-        for j in range(nz - pos - 1, 0, -1):
-            pass_on(pos, j, 1)
+    def stage(k, turns, now=()):
+        h = late(k)
+        for i, t in enumerate(turns + [None]):
+            if t is not None:
+                product(order(t), h)
+            if i > 0:
+                pair(order(turns[i - 1]), h)
+                if turns[i - 1] in now:
+                    leave(order(turns[i - 1]), h)
+
+    if nz > 2:
+        inner(lambda: relay(2, (0,)))
+        hidden(order(2))
+        turn(DN, order(0))
+        arrive(DN[1:], order(1))
+        arrive(DN[:1], late(2))
+        inner(lambda: relay(2, (1,)))
+        hidden(order(1))
+        inner(lambda: relay(2, (2,)))
+        rest(DN, order(0))
+        stage(0, [2, 1], (2, 1))
+        turn(DN, order(1))
+        arrive(DN[1:], late(2))
+        inner(lambda: relay(2, range(3, BITS)))
+        rest(DN, order(1))
+        stage(1, [2, 1], (2, 1))
+        turn(DN, late(2))
+        arrive(DN, late(3))
+        relay(3, range(BITS))
+        hidden(order(3))
+        stage(0, [3], (3,))
+        stage(1, [3], (3,))
+        pass_on(1, 1, 0)
+        pass_on(1, 1, 1)
+        rest(DN, late(2))
+        stage(2, [3, 2, 1], (3, 2))
+        turn(DN, late(3))
+        hidden(order(0))
+        for k in range(3):
+            product(order(0), late(k))
+        pass_on(1, 2, 0)
+        pass_on(1, 2, 1)
+        rest(DN, late(3))
+        stage(3, [3, 2, 1], (3, 2))
+        leave(order(1), late(2))
+        leave(order(1), late(3))
+        product(order(0), late(3))
+        pass_on(2, 1, 0)
+        pass_on(1, 2, 2)
+        pass_on(1, 1, 2)
+        pass_on(2, 1, 1)
+        pass_on(2, 1, 2)
+        pass_on(1, 2, 3)
+        pass_on(1, 1, 3)
+        pass_on(2, 1, 3)
+        for k in range(nz):
+            pair(order(0), order(k))
+    else:
+        hidden(order(1))
+        hidden(order(0))
+        turn(DN, order(0))
+        rest(DN, order(0))
+        stage(0, [1, 0], (1,))
+        arrive(DN, order(1))
+        turn(DN, order(1))
+        rest(DN, order(1))
+        stage(1, [1, 0], (1,))
 
     for way in range(2):
         back = z - 1 + 2 * way
 
         @pl.when(inside(back))
         def _():
-            for h in range(2):
+            for h in range(nz):
                 zc_wait(way, z, h)
 
         @pl.when(jnp.logical_not(inside(back)))
         def _():
             zr[way, z] = jnp.zeros((rows, width), jnp.bfloat16)
 
-    summed = f32(part.at[z, ds(c * rows, rows, rows)]) + f32(zr.at[0, z]) + f32(zr.at[1, z])
-    average = jnp.mean(summed, axis=1, keepdims=True)
-    centered = summed - average
-    variance = jnp.mean(centered * centered, axis=1, keepdims=True)
-    normed = centered * lax.rsqrt(variance + 1e-05) * gain_ref[...] + shift_ref[...]
-    out_ref[...] = normed.astype(out_ref.dtype)
+    def finish():
+        summed = f32(part.at[z, ds(c * rows, rows, rows)]) + f32(zr.at[0, z]) + f32(zr.at[1, z])
+        average = jnp.mean(summed, axis=1, keepdims=True)
+        centered = summed - average
+        variance = jnp.mean(centered * centered, axis=1, keepdims=True)
+        normed = centered * lax.rsqrt(variance + 1e-05) * gain_ref[...] + shift_ref[...]
+        out_ref[...] = normed.astype(out_ref.dtype)
+
+    finish()
 
     for way in range(2):
 
@@ -439,27 +502,31 @@
                     for b in range(BITS):
                         tok_z(chunk(zz, c, b), zz, way, b).wait_send()
 
+                    @pl.when(keeper)
+                    def _():
+                        halo_z(zz, way).wait_send()
+
                 dest = z + (step + 1) * (1 - 2 * way)
 
                 @pl.when(inside(dest))
                 def _():
-                    for h in range(2):
+                    for h in range(nz):
                         zc_copy(way, dest, h).wait_send()
 
     for zz in range(nz):
         for cc in c_others:
             tok_c(slot(zz, c), zz, cc).wait_send()
-            for h in range(2):
+            for h in range(nz):
                 rc_copy(zz, cc, h).wait_send()
 
-        @pl.when((c == nc - 1) & (y < ny - 1))
-        def _():
-            halo_y(tail(zz), zz).wait_send()
-
-        @pl.when((c == nc - 1) & (y > 0))
+        @pl.when(keeper)
         def _():
             for cc in c_others:
                 halo_c(zz, cc).wait_send()
+
+    @pl.when((c == nc - 1) & (y < ny - 1))
+    def _():
+        halo_y().wait_send()
 
     for kind in range(2):
         for yy in y_others:
@@ -517,6 +584,7 @@
                 dma((nz, nc)),
                 dma((nz,)),
                 dma((nz,)),
+                dma((2, nz)),
                 dma((nz, nc)),
                 dma((2, ny)),
                 dma((2, ny)),
@@ -525,10 +593,10 @@
                 dma((4, nz, nx)),
                 dma((4, nz, ny)),
                 dma((4, nz, nx, ny)),
-                dma((nz, 2)),
-                dma((nz, nc, 2)),
-                dma((2, nz, 2)),
-                dma((2, nz, 2)),
+                dma((nz, nz)),
+                dma((nz, nc, nz)),
+                dma((2, nz, nz)),
+                dma((2, nz, nz)),
             ],
             compiler_params=pltpu.CompilerParams(
                 collective_id=0, has_side_effects=True, vmem_limit_bytes=60 * 2**20

time: 142 us -> 121 us (0.85)
  Pallas kernels: 140 us -> 119 us
    pallas_call x1, Pallas kernels: 140 us -> 119 us  [local(): pl.pallas_call(functools.partial(kernel, (nz, nx, ny, nc)), out_shape=jax...]
where the time goes in v2:
time: 121 us
  Pallas kernels  119 us (98%)
  local copies, waits for them, and re-layouts  1.88 us (2%)
    pallas_call x1, Pallas kernels, local(): pl.pallas_call(functools.partial(kernel, (nz, nx, ny, nc)), out_shape=jax...  119 us

profile of v2, /device:TPU:0, one launch (start us, length us, event | category | flops | bytes accessed | tf_op | source)
XLA Modules:
  0.0 121.1 jit_solution(12101854446098723625)
XLA Ops:
  0.0 119.2 %shard_map.82 = bf16[128,2048]{1,0:T(8,128)(2,1)} custom-call(bf16[128,2048]{1,0:T(8,128)(2,1)} %x_ref.1, bf16[256,1536]{1,0:T(8,128)(2,1)} %g_ref.1, bf16[256,1536]{1,0:T(8,128)(2,1)} %v_ref.1, f32[3,1536]{1,0:T(4,128)} %gt_ref.1, f32[3,1536]{1,0:T(4,128)} %vt_ref.1, bf16[1536,256]{1,0:T(8,128)(2,1)} %d_ref.1, f32[1,2048]{1,0:T(1,128)} %bitcast.2, ...), custom_call_target="tpu_custom_call" | custom-call | tf_op jit(solution)/shard_map/pallas_call | solution.py:565
  119.2 1.9 %copy.10 = bf16[128,2048]{1,0:T(8,128)(2,1)} copy(bf16[128,2048]{1,0:T(8,128)(2,1)} %shard_map.82) | data formatting | bytes 1048576

commit v3 on v2

--- a/solution.py
+++ b/solution.py
@@ -16,14 +16,15 @@
 
 def kernel(
     dims,
-    x_ref, g_ref, v_ref, gt_ref, vt_ref, d_ref, gain_ref, shift_ref,
+    x_hbm, g_hbm, v_hbm, gt_hbm, vt_hbm, d_hbm, gain_hbm, shift_hbm,
     out_ref,
+    g_ref, v_ref, tapin, d_ref, gain_ref, shift_ref, in_s,
     tok, gw, vw, dw, taps, pre_g, pre_v, hid, part, rc, zr,
-    tok_r, tz_s, tc_s, halo_r, halo_s, hz_s, hc_s, tap_r, tap_s,
-    w_r, wz_s, wx_s, wy_s, wf_s, rc_r, rc_s, zc_r, zc_s,
+    tok_r, tokc_r, tz_s, tc_s, halo_r, halo_s, hz_s, hc_s, tap_r, tap_s,
+    wl_r, wt_r, wr_r, w_s, rc_r, rc_s, zc_r, zc_s,
 ):
     nz, nx, ny, nc = dims
-    rows, width = x_ref.shape
+    rows, width = x_hbm.shape
     depth = g_ref.shape[0]
     units = gw.shape[1] // ny
     cols = d_ref.shape[1]
@@ -44,6 +45,39 @@
     y_others = [(y + i) % ny for i in range(1, ny)]
     c_others = [(c + i) % nc for i in range(1, nc)]
 
+    def ds(start, size, unit):
+        return pl.ds(pl.multiple_of(start, unit), size)
+
+    mine = ds(fs * depth, depth, depth)
+    here = ds(y * units, units, 128)
+    part_units = ds(z * units, units, 128)
+    moves = [
+        (g_hbm, g_ref, 0),
+        (v_hbm, v_ref, 1),
+        (x_hbm, tok.at[z, ds(HALO + c * rows, rows, 16)], 2),
+        (d_hbm, d_ref, 3),
+        (gt_hbm, tapin.at[0], 4),
+        (vt_hbm, tapin.at[1], 4),
+        (g_hbm.at[:, part_units], gw.at[mine, here], 5),
+        (v_hbm.at[:, part_units], vw.at[mine, here], 5),
+        (d_hbm.at[ds(z * units, units, 16)], dw.at[ds(y * units, units, 16), ds(fs * cols, cols, cols)], 5),
+        (gt_hbm.at[:, part_units], taps.at[0, :, here], 6),
+        (vt_hbm.at[:, part_units], taps.at[1, :, here], 6),
+        (gain_hbm, gain_ref, 7),
+        (shift_hbm, shift_ref, 8),
+    ]
+    for src, dst, i in moves:
+        pltpu.make_async_copy(src, dst, in_s.at[i]).start()
+
+    def loaded(i):
+        whole = [
+            g_ref, v_ref, slot_z, d_ref, tapin, gw.at[pl.ds(0, 3 * depth), pl.ds(0, units)],
+            taps.at[:, :, here], gain_ref, shift_ref,
+        ][i]
+        pltpu.make_async_copy(whole, whole, in_s.at[i]).wait()
+
+    slot_z = tok.at[z, ds(HALO + c * rows, rows, 16)]
+
     barrier = pltpu.get_barrier_semaphore()
     partners = (
         [at(zz=i) for i in z_others]
@@ -61,9 +95,6 @@
             device_id=device, device_id_type=MESH,
         )
 
-    def ds(start, size, unit):
-        return pl.ds(pl.multiple_of(start, unit), size)
-
     half = (2 * z) // nz
     near = z + half * (nz - 1 - 2 * z)
 
@@ -92,14 +123,6 @@
         @pl.when(ends)
         def _():
             act()
-
-    def both(step, act):
-        for way in range(2):
-            zz = z - step + 2 * step * way
-
-            @pl.when(inside(zz))
-            def _():
-                act(zz, way)
 
     def piece(kind, zz):
         if kind >= 2:
@@ -113,33 +136,31 @@
         ref = gw if kind == 0 else vw
         return ref.at[ds(src * depth, depth, depth), ds(yy * units, units, 128)]
 
+    def bulk(kind, a, b):
+        if kind >= 2:
+            return dw.at[pl.ds(0, top * b), pl.ds(0, cols * a)]
+        return gw.at[pl.ds(0, depth * a), pl.ds(0, units * b)]
+
+    def final(kind, zz):
+        return wr_r.at[kind if kind < 2 else 2 + (kind - 2) * nz + zz]
+
+    def await_recv(ref, sem):
+        copy(ref, ref, w_s.at[0, 0], sem, partners[0]).wait_recv()
+
+    def await_send(ref, sem):
+        copy(ref, ref, sem, wl_r.at[0, 0], partners[0]).wait_send()
+
     def w_z(kind, zz):
-        return copy(piece(kind, zz), place(kind, fs, y), wz_s.at[kind, zz], w_r.at[kind, fs, y], at(zz=zz))
-
-    def w_x(kind, src, zz, xx):
-        s = zz * nx + x
-        return copy(src, place(kind, s, y), wx_s.at[kind, zz, xx], w_r.at[kind, s, y], at(xx=xx))
-
-    def w_y(kind, src, zz, yy):
-        s = zz * nx + x
-        return copy(src, place(kind, s, y), wy_s.at[kind, zz, yy], w_r.at[kind, s, y], at(yy=yy))
-
-    def w_f(kind, zz, xx, yy):
-        if kind % 2 == 0:
-            s = zz * nx + xx
-            return copy(place(kind, s, y), place(kind, s, y), wf_s.at[kind, zz, xx, yy], w_r.at[kind, s, y], at(yy=yy))
-        s = zz * nx + x
-        return copy(place(kind, s, yy), place(kind, s, yy), wf_s.at[kind, zz, xx, yy], w_r.at[kind, s, yy], at(xx=xx))
-
-    def w_wait(kind, zz, xx, yy):
-        s = zz * nx + xx
-        copy(place(kind, s, yy), place(kind, s, yy), wz_s.at[kind, 0], w_r.at[kind, s, yy], partners[0]).wait_recv()
+        return copy(piece(kind, zz), place(kind, fs, y), w_s.at[kind, 0], wl_r.at[kind // 2, z], at(zz=zz))
 
     def spread(kind, src, zz):
-        for xx in x_others:
-            w_x(kind, src, zz, xx).start()
-        for yy in y_others:
-            w_y(kind, src, zz, yy).start()
+        dst = place(kind, zz * nx + x, y)
+        for i, xx in enumerate(x_others):
+            recv = wt_r.at[kind, zz, nx - i - 2] if kind % 2 == 0 else final(kind, zz)
+            copy(src, dst, w_s.at[kind, 1], recv, at(xx=xx)).start()
+        for i, yy in enumerate(y_others):
+            recv = wt_r.at[kind, zz, ny - i - 2] if kind % 2 == 1 else final(kind, zz)
+            copy(src, dst, w_s.at[kind, 2], recv, at(yy=yy)).start()
 
     def own(kinds):
         for kind in kinds:
@@ -147,33 +168,26 @@
 
     def arrive(kinds, zz):
         for kind in kinds:
-            w_wait(kind, zz, x, y)
+            if kind % 2 == 0:
+                await_recv(bulk(kind, 2, 1) if kind < 2 else bulk(kind, 1, 2), wl_r.at[kind // 2, zz])
             spread(kind, place(kind, zz * nx + x, y), zz)
 
     def turn(kinds, zz):
         for kind in kinds:
-            if kind % 2 == 0:
-                for xx in x_others:
-                    w_wait(kind, zz, xx, y)
-                    for yy in y_others:
-                        w_f(kind, zz, xx, yy).start()
-            else:
-                for yy in y_others:
-                    w_wait(kind, zz, x, yy)
-                    for xx in x_others:
-                        w_f(kind, zz, xx, yy).start()
+            across, along = (x_others, y_others) if kind % 2 == 0 else (y_others, x_others)
+            for i, a in enumerate(across):
+                ref = place(kind, zz * nx + a, y) if kind % 2 == 0 else place(kind, zz * nx + x, a)
+                await_recv(ref, wt_r.at[kind, zz, i])
+                for b in along:
+                    device = at(yy=b) if kind % 2 == 0 else at(xx=b)
+                    copy(ref, ref, w_s.at[kind, 3], final(kind, zz), device).start()
 
     def rest(kinds, zz):
         for kind in kinds:
-            if kind % 2 == 0:
-                for yy in y_others:
-                    w_wait(kind, zz, x, yy)
-            else:
-                for xx in x_others:
-                    w_wait(kind, zz, xx, y)
-            for xx in x_others:
-                for yy in y_others:
-                    w_wait(kind, zz, xx, yy)
+            a = nx if kind % 2 == 0 else nx - 1
+            b = ny - 1 if kind % 2 == 0 else ny
+            if a and b:
+                await_recv(bulk(kind, a * nz if kind < 2 else a, b), final(kind, zz))
 
     def slot(zz, cc):
         return tok.at[zz, ds(HALO + cc * rows, rows, 16)]
@@ -182,10 +196,10 @@
         return tok.at[zz, ds(HALO + cc * rows + b * bit, bit, 16)]
 
     def tok_z(src, zz, way, b):
-        return copy(src, chunk(zz, c, b), tz_s.at[way, zz, b], tok_r.at[zz, c, b], at(zz=z + 1 - 2 * way))
+        return copy(src, chunk(zz, c, b), tz_s.at[way], tok_r.at[zz, b], at(zz=z + 1 - 2 * way))
 
     def tok_c(src, zz, cc):
-        return copy(src, slot(zz, c), tc_s.at[zz, cc], tok_r.at[zz, c, 0], at(cc=cc))
+        return copy(src, slot(zz, c), tc_s.at[0], tokc_r.at[zz], at(cc=cc))
 
     keeper = (c == nc - 1) & (y > 0)
 
@@ -193,16 +207,16 @@
         return tok.at[zz, pl.ds(0, HALO)]
 
     def halo_y():
-        return copy(x_ref.at[pl.ds(rows - HALO, HALO)], lead(z), halo_s.at[z], halo_r.at[z], at(yy=y + 1))
+        return copy(tok.at[z, ds(c * rows + rows, HALO, 16)], lead(z), halo_s.at[0], halo_r.at[z], at(yy=y + 1))
 
     def halo_z(zz, way):
-        return copy(lead(zz), lead(zz), hz_s.at[way, zz], halo_r.at[zz], at(zz=z + 1 - 2 * way))
+        return copy(lead(zz), lead(zz), hz_s.at[way], halo_r.at[zz], at(zz=z + 1 - 2 * way))
 
     def halo_c(zz, cc):
-        return copy(lead(zz), lead(zz), hc_s.at[zz, cc], halo_r.at[zz], at(cc=cc))
+        return copy(lead(zz), lead(zz), hc_s.at[0], halo_r.at[zz], at(cc=cc))
 
     def halo_wait(zz):
-        copy(lead(zz), lead(zz), hc_s.at[zz, 0], halo_r.at[zz], partners[0]).wait_recv()
+        await_recv(lead(zz), halo_r.at[zz])
 
     def keep(zz, ways, further):
         @pl.when(keeper)
@@ -230,7 +244,7 @@
             @pl.when(inside(zz))
             def _():
                 for b in bits:
-                    copy(chunk(zz, c, b), chunk(zz, c, b), tz_s.at[0, 0, 0], tok_r.at[zz, c, b], partners[0]).wait_recv()
+                    await_recv(chunk(zz, c, b), tok_r.at[zz, b])
                     if step < nz - 1:
 
                         @pl.when(inside(ahead))
@@ -243,22 +257,17 @@
 
     def gathered(zz):
         for cc in c_others:
-            copy(slot(zz, cc), slot(zz, cc), tz_s.at[0, 0, 0], tok_r.at[zz, cc, 0], partners[0]).wait_recv()
+            await_recv(slot(zz, cc), tokc_r.at[zz])
 
         @pl.when((y > 0) & (c < nc - 1))
         def _():
             halo_wait(zz)
 
     def tap(kind, yy):
-        ref = gt_ref if kind == 0 else vt_ref
-        return copy(
-            ref.at[:, ds(z * units, units, 128)], taps.at[kind, :, ds(y * units, units, 128)],
-            tap_s.at[kind, yy], tap_r.at[kind, y], at(yy=yy),
-        )
-
-    def tap_wait(kind, yy):
-        dst = taps.at[kind, :, ds(yy * units, units, 128)]
-        copy(dst, dst, tap_s.at[kind, yy], tap_r.at[kind, yy], partners[0]).wait_recv()
+        return copy(tapin.at[kind, :, part_units], taps.at[kind, :, here], tap_s.at[0], tap_r.at[0], at(yy=yy))
+
+    def tap_bulk():
+        return taps.at[:, :, pl.ds(0, units * (ny - 1))]
 
     def place_of(way):
         return z + way * (nz - 1 - 2 * z)
@@ -274,49 +283,49 @@
 
     central = nz // 2 - 1
 
-    @pl.when((c == nc - 1) & (y < ny - 1))
-    def _():
-        halo_y().start()
-
+    loaded(0)
+    loaded(1)
     own(GV)
     for way in range(2):
         pos = place_of(way)
         line(GV, way, (1,), pos == 0)
         line(GV, way, range(nz - 1, 0, -1), pos > 0)
+    loaded(2)
+
+    @pl.when((c == nc - 1) & (y < ny - 1))
+    def _():
+        halo_y().start()
+
+    for way in range(2):
+        pos = place_of(way)
 
         @pl.when(inside(z + 1 - 2 * way))
         def _():
             for b in range(BITS):
-                tok_z(x_ref.at[pl.ds(b * bit, bit)], z, way, b).start()
+                tok_z(chunk(z, c, b), z, way, b).start()
 
         line(GV, way, range(nz - 1, 1, -1), pos == 0)
-        line(DN, way, (1,), pos != central)
+    loaded(3)
+    loaded(4)
+    for way in range(2):
+        line(DN, way, (1,), place_of(way) != central)
     for kind in range(2):
         for yy in y_others:
             tap(kind, yy).start()
-    cross(x_ref, z)
+    cross(slot(z, c), z)
 
     @pl.when(y == 0)
     def _():
         tok[:, 0:HALO, :] = jnp.zeros((nz, HALO, width), jnp.bfloat16)
 
-    tok[z, ds(HALO + c * rows, rows, 16)] = x_ref[...]
-    mine = ds(fs * depth, depth, depth)
-    here = ds(y * units, units, 128)
-    part_units = ds(z * units, units, 128)
-    gw[mine, here] = g_ref[:, part_units]
-    vw[mine, here] = v_ref[:, part_units]
-    dw[here, ds(fs * cols, cols, cols)] = d_ref[part_units, :]
-    taps[0, :, here] = gt_ref[:, part_units]
-    taps[1, :, here] = vt_ref[:, part_units]
-
     keep(z, range(2), True)
     side = nz // 2
     for k in range(1, nz):
-        if k == nz - 1:
+        first = k in (1, nz - 1)
+        if first:
             turn(GV, early(k - 1))
         arrive(GV, early(k))
-        if k < nz - 1:
+        if not first:
             turn(GV, early(k - 1))
     relay(1, range(BITS))
     for way in range(2):
@@ -328,11 +337,11 @@
     if nz > 2:
         arrive(DN[:1], order(1))
         outer(lambda: relay(2, range(BITS)))
-    for kind in range(2):
-        for yy in y_others:
-            tap_wait(kind, yy)
-    for k in range(nz):
-        rest(GV, order(k))
+    for i in range(5, 9):
+        loaded(i)
+    if ny > 1:
+        await_recv(tap_bulk(), tap_r.at[0])
+    rest(GV, 0)
 
     def f32(ref):
         return ref[...].astype(jnp.float32)
@@ -360,14 +369,15 @@
         return part.at[zz, ds(cc * rows, rows, rows), wing(h)]
 
     def rc_copy(zz, cc, h):
-        return copy(block(zz, cc, h), rc.at[zz, :, wing(h)], rc_s.at[zz, cc, h], rc_r.at[zz, h], at(cc=cc))
+        return copy(block(zz, cc, h), rc.at[zz, :, wing(h)], rc_s.at[0], rc_r.at[zz, h], at(cc=cc))
 
     def zc_copy(way, zz, h):
-        return copy(block(zz, c, h), zr.at[way, zz, :, wing(h)], zc_s.at[way, zz, h], zc_r.at[way, zz, h], at(zz=z + 1 - 2 * way))
+        ahead = z + 1 - 2 * way
+        recv = zc_r.at[jnp.where(zz == ahead, nz * nz + way, zz * nz + h)]
+        return copy(block(zz, c, h), zr.at[way, zz, :, wing(h)], zc_s.at[way], recv, at(zz=ahead))
 
     def zc_wait(way, zz, h):
-        dst = zr.at[way, zz, :, wing(h)]
-        copy(dst, dst, zc_s.at[way, zz, h], zc_r.at[way, zz, h], partners[0]).wait_recv()
+        await_recv(zr.at[way, zz, :, wing(h)], zc_r.at[zz * nz + h])
 
     def product(zz, h):
         part[zz, :, wing(h)] = jnp.dot(
@@ -415,14 +425,13 @@
         hidden(order(2))
         turn(DN, order(0))
         arrive(DN[1:], order(1))
-        arrive(DN[:1], late(2))
         inner(lambda: relay(2, (1,)))
         hidden(order(1))
         inner(lambda: relay(2, (2,)))
         rest(DN, order(0))
         stage(0, [2, 1], (2, 1))
         turn(DN, order(1))
-        arrive(DN[1:], late(2))
+        arrive(DN, late(2))
         inner(lambda: relay(2, range(3, BITS)))
         rest(DN, order(1))
         stage(1, [2, 1], (2, 1))
@@ -469,12 +478,43 @@
         stage(1, [1, 0], (1,))
 
     for way in range(2):
+        for p in range(nz - 1):
+
+            @pl.when(place_of(way) == p)
+            def _():
+                await_send(part.at[pl.ds(0, p + 1), pl.ds(0, rows)], tz_s.at[way])
+                await_send(part.at[pl.ds(0, nz - 1 - p), pl.ds(0, rows)], zc_s.at[way])
+
+                @pl.when(keeper)
+                def _():
+                    await_send(part.at[pl.ds(0, p + 1), pl.ds(0, HALO)], hz_s.at[way])
+
+    @pl.when((c == nc - 1) & (y < ny - 1))
+    def _():
+        await_send(lead(z), halo_s.at[0])
+
+    if nc > 1:
+        others = part.at[:, pl.ds(0, rows * (nc - 1))]
+        await_send(others, tc_s.at[0])
+        await_send(others, rc_s.at[0])
+
+        @pl.when(keeper)
+        def _():
+            await_send(part.at[:, pl.ds(0, HALO * (nc - 1))], hc_s.at[0])
+
+    if ny > 1:
+        await_send(tap_bulk(), tap_s.at[0])
+    for kind in GV + DN:
+        for way, (a, b) in enumerate([(nz - 1, 1), (nz * (nx - 1), 1), (nz, ny - 1), (nz * (nx - 1), ny - 1)]):
+            if a and b:
+                await_send(bulk(kind, a, b), w_s.at[kind, way])
+
+    for way in range(2):
         back = z - 1 + 2 * way
 
         @pl.when(inside(back))
         def _():
-            for h in range(nz):
-                zc_wait(way, z, h)
+            await_recv(zr.at[way, z], zc_r.at[nz * nz + way])
 
         @pl.when(jnp.logical_not(inside(back)))
         def _():
@@ -489,60 +529,6 @@
         out_ref[...] = normed.astype(out_ref.dtype)
 
     finish()
-
-    for way in range(2):
-
-        @pl.when(inside(z + 1 - 2 * way))
-        def _():
-            for step in range(nz - 1):
-                zz = z - step + 2 * step * way
-
-                @pl.when(inside(zz))
-                def _():
-                    for b in range(BITS):
-                        tok_z(chunk(zz, c, b), zz, way, b).wait_send()
-
-                    @pl.when(keeper)
-                    def _():
-                        halo_z(zz, way).wait_send()
-
-                dest = z + (step + 1) * (1 - 2 * way)
-
-                @pl.when(inside(dest))
-                def _():
-                    for h in range(nz):
-                        zc_copy(way, dest, h).wait_send()
-
-    for zz in range(nz):
-        for cc in c_others:
-            tok_c(slot(zz, c), zz, cc).wait_send()
-            for h in range(nz):
-                rc_copy(zz, cc, h).wait_send()
-
-        @pl.when(keeper)
-        def _():
-            for cc in c_others:
-                halo_c(zz, cc).wait_send()
-
-    @pl.when((c == nc - 1) & (y < ny - 1))
-    def _():
-        halo_y().wait_send()
-
-    for kind in range(2):
-        for yy in y_others:
-            tap(kind, yy).wait_send()
-    for kind in GV + DN:
-        for zz in z_others:
-            w_z(kind, zz).wait_send()
-        for zz in range(nz):
-            src = place(kind, zz * nx + x, y)
-            for xx in x_others:
-                w_x(kind, src, zz, xx).wait_send()
-            for yy in y_others:
-                w_y(kind, src, zz, yy).wait_send()
-            for xx in x_others:
-                for yy in y_others:
-                    w_f(kind, zz, xx, yy).wait_send()
 
 
 def solution(mesh):
@@ -564,10 +550,17 @@
         dma = pltpu.SemaphoreType.DMA
         return pl.pallas_call(
             functools.partial(kernel, (nz, nx, ny, nc)),
-            out_shape=jax.ShapeDtypeStruct((rows, width), bf16),
-            in_specs=[pl.BlockSpec(memory_space=pltpu.VMEM)] * 8,
+            out_shape=pltpu.VMEM((rows, width), bf16),
+            in_specs=[pl.BlockSpec(memory_space=pltpu.HBM)] * 8,
             out_specs=pl.BlockSpec(memory_space=pltpu.VMEM),
             scratch_shapes=[
+                pltpu.VMEM((depth, held), bf16),
+                pltpu.VMEM((depth, held), bf16),
+                pltpu.VMEM((2, count, held), jnp.float32),
+                pltpu.VMEM(down_weight.shape, bf16),
+                pltpu.VMEM((1, width), jnp.float32),
+                pltpu.VMEM((1, width), jnp.float32),
+                dma((9,)),
                 pltpu.VMEM((nz, HALO + length, width), bf16),
                 pltpu.VMEM((width, ny * units), bf16),
                 pltpu.VMEM((width, ny * units), bf16),
@@ -579,27 +572,27 @@
                 pltpu.VMEM((nz, length, width), bf16),
                 pltpu.VMEM((nz, rows, width), bf16),
                 pltpu.VMEM((2, nz, rows, width), bf16),
-                dma((nz, nc, BITS)),
-                dma((2, nz, BITS)),
-                dma((nz, nc)),
+                dma((nz, BITS)),
                 dma((nz,)),
+                dma((2,)),
+                dma((1,)),
                 dma((nz,)),
+                dma((1,)),
+                dma((2,)),
+                dma((1,)),
+                dma((1,)),
+                dma((1,)),
                 dma((2, nz)),
-                dma((nz, nc)),
-                dma((2, ny)),
-                dma((2, ny)),
-                dma((4, n_fs, ny)),
-                dma((4, nz)),
-                dma((4, nz, nx)),
-                dma((4, nz, ny)),
-                dma((4, nz, nx, ny)),
+                dma((4, nz, max(nx, ny, 2) - 1)),
+                dma((2 + 2 * nz,)),
+                dma((4, 4)),
                 dma((nz, nz)),
-                dma((nz, nc, nz)),
-                dma((2, nz, nz)),
-                dma((2, nz, nz)),
+                dma((1,)),
+                dma((nz * nz + 2,)),
+                dma((2,)),
             ],
             compiler_params=pltpu.CompilerParams(
-                collective_id=0, has_side_effects=True, vmem_limit_bytes=60 * 2**20
+                collective_id=0, has_side_effects=True, vmem_limit_bytes=58 * 2**20
             ),
         )(
             tokens, gate_weight, value_weight, gate_taps, value_taps, down_weight,

time: 121 us -> 115 us (0.950)
  Pallas kernels: 119 us -> 114 us
    pallas_call x1, Pallas kernels: 119 us -> 114 us  [local(): pl.pallas_call(functools.partial(kernel, (nz, nx, ny, nc)), out_shape=plt...]
where the time goes in v3:
time: 115 us
  Pallas kernels  114 us (99%)
    pallas_call x1, Pallas kernels, local(): pl.pallas_call(functools.partial(kernel, (nz, nx, ny, nc)), out_shape=plt...  114 us

profile of v3, /device:TPU:0, one launch (start us, length us, event | category | flops | bytes accessed | tf_op | source)
XLA Modules:
  0.0 114.6 jit_solution(18229012284912791869)
XLA Ops:
  0.0 113.8 %shard_map.82 = bf16[128,2048]{1,0:T(8,128)(2,1)S(1)} custom-call(bf16[128,2048]{1,0:T(8,128)(2,1)} %x_hbm.1, bf16[256,1536]{1,0:T(8,128)(2,1)} %g_hbm.1, bf16[256,1536]{1,0:T(8,128)(2,1)} %v_hbm.1, f32[3,1536]{1,0:T(4,128)} %gt_hbm.1, f32[3,1536]{1,0:T(4,128)} %vt_hbm.1, bf16[1536,256]{1,0:T(8,128)(2,1)} %d_hbm.1, f32[1,2048]{1,0:T(1,128)} %bitcast.2, ...), custom_call_target="tpu_custom_call" | custom-call | tf_op jit(solution)/shard_map/pallas_call | solution.py:551
  113.8 0.8 copy.10

commit v4 on v3

--- a/solution.py
+++ b/solution.py
@@ -19,7 +19,7 @@
     x_hbm, g_hbm, v_hbm, gt_hbm, vt_hbm, d_hbm, gain_hbm, shift_hbm,
     out_ref,
     g_ref, v_ref, tapin, d_ref, gain_ref, shift_ref, in_s,
-    tok, gw, vw, dw, taps, pre_g, pre_v, hid, part, rc, zr,
+    tok, gw, vw, dw, taps, pre_g, pre_v, hid, part, rc, zr, zx,
     tok_r, tokc_r, tz_s, tc_s, halo_r, halo_s, hz_s, hc_s, tap_r, tap_s,
     wl_r, wt_r, wr_r, w_s, rc_r, rc_s, zc_r, zc_s,
 ):
@@ -329,7 +329,7 @@
             turn(GV, early(k - 1))
     relay(1, range(BITS))
     for way in range(2):
-        line(DN, way, range(nz - 1, 0, -1), place_of(way) == central)
+        line(DN, way, range(1, nz), place_of(way) == central)
     turn(GV, order(nz - 1))
     own(DN)
     for way in range(2):
@@ -397,7 +397,10 @@
         def _():
             zc_copy(half, zz, h).start()
 
-    def pass_on(pos, j, e):
+    def zx_copy(way, zz, h):
+        return copy(block(zz, c, h), zx, zc_s.at[way], zc_r.at[nz * nz + 2], at(zz=zz))
+
+    def pass_on(pos, j, e, add=True, skip=False):
         way = jnp.where(z == pos, 0, 1)
         dest = z + j * (1 - 2 * way)
         e = 5 - e if e > 1 else e
@@ -405,10 +408,11 @@
 
         @pl.when((z == pos) | (z == nz - 1 - pos))
         def _():
-            zc_wait(way, dest, h)
-            sent = block(dest, c, h)
-            sent[...] = (f32(sent) + f32(zr.at[way, dest, :, wing(h)])).astype(jnp.bfloat16)
-            zc_copy(way, dest, h).start()
+            if add:
+                zc_wait(way, dest, h)
+                sent = block(dest, c, h)
+                sent[...] = (f32(sent) + f32(zr.at[way, dest, :, wing(h)])).astype(jnp.bfloat16)
+            (zx_copy if skip else zc_copy)(way, dest, h).start()
 
     def stage(k, turns, now=()):
         h = late(k)
@@ -436,11 +440,12 @@
         rest(DN, order(1))
         stage(1, [2, 1], (2, 1))
         turn(DN, late(2))
+        relay(3, range(BITS))
         arrive(DN, late(3))
-        relay(3, range(BITS))
         hidden(order(3))
         stage(0, [3], (3,))
         stage(1, [3], (3,))
+        pass_on(2, 1, 3, add=False)
         pass_on(1, 1, 0)
         pass_on(1, 1, 1)
         rest(DN, late(2))
@@ -460,10 +465,9 @@
         pass_on(1, 2, 2)
         pass_on(1, 1, 2)
         pass_on(2, 1, 1)
+        pass_on(1, 2, 3, skip=True)
         pass_on(2, 1, 2)
-        pass_on(1, 2, 3)
         pass_on(1, 1, 3)
-        pass_on(2, 1, 3)
         for k in range(nz):
             pair(order(0), order(k))
     else:
@@ -520,6 +524,14 @@
         def _():
             zr[way, z] = jnp.zeros((rows, width), jnp.bfloat16)
 
+    if nz > 2:
+
+        @pl.when(ends)
+        def _():
+            await_recv(zx, zc_r.at[nz * nz + 2])
+            last = zr.at[1 - half, z, :, wing(1 + half)]
+            last[...] = (f32(last) + f32(zx)).astype(jnp.bfloat16)
+
     def finish():
         summed = f32(part.at[z, ds(c * rows, rows, rows)]) + f32(zr.at[0, z]) + f32(zr.at[1, z])
         average = jnp.mean(summed, axis=1, keepdims=True)
@@ -545,6 +557,7 @@
             nz //= 2
         nx = n_fs // nz
         units = held // nz
+        cols = down_weight.shape[1]
         length = nc * rows
         bf16 = jnp.bfloat16
         dma = pltpu.SemaphoreType.DMA
@@ -572,6 +585,7 @@
                 pltpu.VMEM((nz, length, width), bf16),
                 pltpu.VMEM((nz, rows, width), bf16),
                 pltpu.VMEM((2, nz, rows, width), bf16),
+                pltpu.VMEM((rows, nx * cols), bf16),
                 dma((nz, BITS)),
                 dma((nz,)),
                 dma((2,)),
@@ -588,7 +602,7 @@
                 dma((4, 4)),
                 dma((nz, nz)),
                 dma((1,)),
-                dma((nz * nz + 2,)),
+                dma((nz * nz + 3,)),
                 dma((2,)),
             ],
             compiler_params=pltpu.CompilerParams(

time: 115 us -> 111 us (0.965)
  Pallas kernels: 114 us -> 110 us
    pallas_call x1, Pallas kernels: 114 us -> 110 us  [local(): pl.pallas_call(functools.partial(kernel, (nz, nx, ny, nc)), out_shape=plt...]
where the time goes in v4:
time: 111 us
  Pallas kernels  110 us (99%)
    pallas_call x1, Pallas kernels, local(): pl.pallas_call(functools.partial(kernel, (nz, nx, ny, nc)), out_shape=plt...  110 us

profile of v4, /device:TPU:0, one launch (start us, length us, event | category | flops | bytes accessed | tf_op | source)
XLA Modules:
  0.0 111.1 jit_solution(8437305295006963345)
XLA Ops:
  0.0 110.3 %shard_map.82 = bf16[128,2048]{1,0:T(8,128)(2,1)S(1)} custom-call(bf16[128,2048]{1,0:T(8,128)(2,1)} %x_hbm.1, bf16[256,1536]{1,0:T(8,128)(2,1)} %g_hbm.1, bf16[256,1536]{1,0:T(8,128)(2,1)} %v_hbm.1, f32[3,1536]{1,0:T(4,128)} %gt_hbm.1, f32[3,1536]{1,0:T(4,128)} %vt_hbm.1, bf16[1536,256]{1,0:T(8,128)(2,1)} %d_hbm.1, f32[1,2048]{1,0:T(1,128)} %bitcast.2, ...), custom_call_target="tpu_custom_call" | custom-call | tf_op jit(solution)/shard_map/pallas_call | solution.py:564
  110.3 0.8 copy.10

commit v5 on v4

--- a/solution.py
+++ b/solution.py
@@ -251,8 +251,10 @@
                         def _():
                             tok_z(chunk(zz, c, b), zz, way, b).start()
 
+                    for cc in c_others:
+                        copy(chunk(zz, c, b), chunk(zz, c, b), tc_s.at[0], tokc_r.at[zz], at(cc=cc)).start()
+
                 if bits[-1] == BITS - 1:
-                    cross(slot(zz, c), zz)
                     keep(zz, (way,), step < nz - 1)
 
     def gathered(zz):
@@ -443,8 +445,11 @@
         relay(3, range(BITS))
         arrive(DN, late(3))
         hidden(order(3))
-        stage(0, [3], (3,))
-        stage(1, [3], (3,))
+        for k in range(2):
+            product(order(3), late(k))
+        for k in range(2):
+            pair(order(3), late(k))
+            leave(order(3), late(k))
         pass_on(2, 1, 3, add=False)
         pass_on(1, 1, 0)
         pass_on(1, 1, 1)

time: 111 us -> 111 us (level)
  no operation moved by 1% of the time
where the time goes in v5:
time: 111 us
  Pallas kernels  110 us (99%)
    pallas_call x1, Pallas kernels, local(): pl.pallas_call(functools.partial(kernel, (nz, nx, ny, nc)), out_shape=plt...  110 us

profile of v5, /device:TPU:0, one launch (start us, length us, event | category | flops | bytes accessed | tf_op | source)
XLA Modules:
  0.0 111.2 jit_solution(13102495983505425944)
XLA Ops:
  0.0 110.4 %shard_map.82 = bf16[128,2048]{1,0:T(8,128)(2,1)S(1)} custom-call(bf16[128,2048]{1,0:T(8,128)(2,1)} %x_hbm.1, bf16[256,1536]{1,0:T(8,128)(2,1)} %g_hbm.1, bf16[256,1536]{1,0:T(8,128)(2,1)} %v_hbm.1, f32[3,1536]{1,0:T(4,128)} %gt_hbm.1, f32[3,1536]{1,0:T(4,128)} %vt_hbm.1, bf16[1536,256]{1,0:T(8,128)(2,1)} %d_hbm.1, f32[1,2048]{1,0:T(1,128)} %bitcast.2, ...), custom_call_target="tpu_custom_call" | custom-call | tf_op jit(solution)/shard_map/pallas_call | solution.py:569
  110.4 0.8 copy.10
